TPU v7x, 32 devices: a whole 2x2x4 slice. The times are simulated.
32 devices in a mesh: ep: 8 (over z, core), tp: 4 (over y, x).
Axes of the slice: x: 2, y: 2, z: 4, core: 2. Of those that a mesh axis runs over, the one named last changes fastest.
Arguments:
- mixer_input: bfloat16 [2048, 2048], P('ep'), may hold values from -6 to 6
- mixer_gain: float32 [2048], replicated, may hold values from 0.1 to 1.9
- query_weight: bfloat16 [2048, 2048], P(None, 'tp'), may hold values from -0.13258252 to 0.13258252
- key_weight: bfloat16 [2048, 1024], P(None, 'tp'), may hold values from -2.78423295 to 2.78423295
- value_weight: bfloat16 [2048, 1024], P(None, 'tp'), may hold values from -0.125 to 0.125
- output_weight: bfloat16 [2048, 2048], P(None, 'tp'), may hold values from -1 to 1
- sink_logit: float32 [32], P('tp'), may hold values from 2 to 7
- expert_input: bfloat16 [1024, 2048], P('ep'), may hold values from -6 to 6
- expert_gain: float32 [2048], replicated, may hold values from 0.1 to 1.9
- routes: int32 [1024, 4], P('ep'), may hold values from 0 to 7, all different within a row; in each aligned block of 128 rows (0 to 127, 128 to 255, ...) at most 128 rows name the same one
- route_logits: float32 [1024, 4], P('ep'), may hold values from -6 to 6
- gate_weight: bfloat16 [8, 2048, 2048], P('ep', None, 'tp'), may hold values from -0.375 to 0.375
- up_weight: bfloat16 [8, 2048, 2048], P('ep', None, 'tp'), may hold values from -0.375 to 0.375
- down_weight: bfloat16 [8, 2048, 2048], P('ep', None, 'tp'), may hold values from -0.03125 to 0.03125
Outputs:
- mixer_output: bfloat16 [2048, 2048], P('ep', 'tp')
- expert_output: bfloat16 [1024, 2048], P('ep', 'tp')
Inputs may be any that keep to these rules, and one draw needn't show every extreme that they name: `routes`: each token names 4 different experts. Among the 128 tokens of one index of ep (aligned blocks) no expert is named more than 128 times, and in some blocks one expert is named exactly 128 times.
All inputs are finite; a program needn't handle non-finite values.
Results may differ from a plain program's by a relative error of at most 0.0055.
The roundings to bfloat16 on the way count: a program that leaves them out, or rounds other values in their place, can miss the bound.
Values may be sent and summed in bfloat16 or wider, within the bound.
A program may use at most 64 MiB of HBM per device.

v0:
```python
import jax
import jax.numpy as jnp
from jax import lax
from jax.sharding import PartitionSpec as P

HEAD_DIM = 64
TOP_K = 4
WINDOW = 128
GRID_W = 64
EPSILON = 1e-06
LIMIT = 7.0
SLOPE = 1.702
BASE = 10000.0


def extended(shard, sides, width):
    for axis, dim in sides:
        devices, length = (lax.axis_size(axis), shard.shape[dim])
        up = [(i, (i + 1) % devices) for i in range(devices - 1)]
        down = [(j, i) for i, j in up]
        last = lax.slice_in_dim(shard, length - width, length, axis=dim)
        first = lax.slice_in_dim(shard, 0, width, axis=dim)
        before = lax.ppermute(last, axis, up)
        after = lax.ppermute(first, axis, down)
        shard = jnp.concatenate([before, shard, after], axis=dim)
    return shard


def normalize(rows, gain):
    values = rows.astype(jnp.float32)
    scaled = values * lax.rsqrt(jnp.mean(values * values, axis=-1, keepdims=True) + EPSILON)
    return (scaled * gain).astype(jnp.bfloat16)


def turn(values, cosine, sine):
    first, second = jnp.split(values, 2, axis=-1)
    cosine = cosine[:, None, :]
    sine = sine[:, None, :]
    return jnp.concatenate(
        [first * cosine - second * sine, second * cosine + first * sine], axis=-1
    )


def axial_rope(values, places):
    quarter = values.shape[-1] // 4
    frequency = BASE ** (-jnp.arange(quarter, dtype=jnp.float32) / quarter)
    row_angle = (places // GRID_W).astype(jnp.float32)[:, None] * frequency[None, :]
    column_angle = (places % GRID_W).astype(jnp.float32)[:, None] * frequency[None, :]
    row_part, column_part = jnp.split(values, 2, axis=-1)
    return jnp.concatenate(
        [
            turn(row_part, jnp.cos(row_angle), jnp.sin(row_angle)),
            turn(column_part, jnp.cos(column_angle), jnp.sin(column_angle)),
        ],
        axis=-1,
    )


def activate(gate, up):
    capped = jnp.minimum(gate, LIMIT)
    bounded = jnp.clip(up, -LIMIT, LIMIT)
    return (capped * jax.nn.sigmoid(SLOPE * capped) * (bounded + 1.0)).astype(jnp.bfloat16)


def add_product(piece, weight):
    return jnp.dot(piece, weight, preferred_element_type=jnp.float32)


def shards(
    mixer_input,
    mixer_gain,
    query_weight,
    key_weight,
    value_weight,
    output_weight,
    sink_logit,
    expert_input,
    expert_gain,
    routes,
    route_logits,
    gate_weight,
    up_weight,
    down_weight,
):
    tokens = mixer_input.shape[0]
    query_heads = query_weight.shape[1] // HEAD_DIM
    key_heads = key_weight.shape[1] // HEAD_DIM
    group = query_heads // key_heads
    blocks = tokens // WINDOW
    offset = lax.axis_index("ep") * tokens
    length = lax.axis_size("ep") * tokens
    places = offset + jnp.arange(tokens, dtype=jnp.int32)
    normed = normalize(mixer_input, mixer_gain)
    query = jnp.dot(normed, query_weight, preferred_element_type=jnp.float32).reshape(
        tokens, query_heads, HEAD_DIM
    )
    query = (
        axial_rope(query, places)
        .astype(jnp.bfloat16)
        .reshape(blocks, WINDOW, key_heads, group, HEAD_DIM)
    )
    keys = jnp.dot(normed, key_weight, preferred_element_type=jnp.float32).reshape(
        tokens, key_heads, HEAD_DIM
    )
    keys = axial_rope(keys, places).astype(jnp.bfloat16).reshape(tokens, key_heads * HEAD_DIM)
    values = jnp.dot(normed, value_weight, preferred_element_type=jnp.float32).astype(jnp.bfloat16)
    stacked = jnp.concatenate([keys, values], axis=1)
    widened = extended(stacked, (("ep", 0),), WINDOW)
    framed = widened.reshape(blocks + 2, WINDOW, 2, key_heads, HEAD_DIM)
    nearby = jnp.concatenate([framed[:-2], framed[1:-1], framed[2:]], axis=1)
    scores = jnp.einsum(
        "nqgrd,nkgd->ngrqk", query, nearby[:, :, 0], preferred_element_type=jnp.float32
    ) * HEAD_DIM ** (-0.5)
    query_place = places.reshape(blocks, WINDOW)
    key_place = (
        offset
        + (jnp.arange(blocks, dtype=jnp.int32)[:, None] - 1) * WINDOW
        + jnp.arange(3 * WINDOW, dtype=jnp.int32)[None, :]
    )
    allowed = (
        (jnp.abs(query_place[:, :, None] - key_place[:, None, :]) <= WINDOW)
        & (key_place[:, None, :] >= 0)
        & (key_place[:, None, :] < length)
    )
    scores = jnp.where(allowed[:, None, None], scores, -1e30)
    sinks = sink_logit.reshape(key_heads, group)[None, :, :, None]
    top = jnp.maximum(jnp.max(scores, axis=-1), sinks)
    weights = jnp.exp(scores - top[..., None])
    denominator = jnp.sum(weights, axis=-1) + jnp.exp(sinks - top)
    shares = (weights / denominator[..., None]).astype(jnp.bfloat16)
    mixed = jnp.einsum(
        "ngrqk,nkgd->nqgrd", shares, nearby[:, :, 1], preferred_element_type=jnp.float32
    )
    mixed = mixed.astype(jnp.bfloat16).reshape(tokens, query_heads * HEAD_DIM)
    experts = lax.axis_size("ep")
    rows_here = expert_input.shape[0]
    capacity = 2 * rows_here * TOP_K // experts
    expert_normed = normalize(expert_input, expert_gain)
    chances = jax.nn.softmax(route_logits, axis=-1)
    chosen = routes.reshape(-1)
    marks = (chosen[:, None] == jnp.arange(experts, dtype=jnp.int32)[None, :]).astype(jnp.int32)
    earlier = jnp.sum((jnp.cumsum(marks, axis=0) - marks) * marks, axis=1)
    target = chosen * capacity + earlier
    source = (
        jnp.full((experts * capacity,), rows_here, jnp.int32)
        .at[target]
        .set(jnp.arange(chosen.shape[0], dtype=jnp.int32) // TOP_K)
    )
    padded = jnp.concatenate(
        [expert_normed, jnp.zeros((1, expert_normed.shape[1]), jnp.bfloat16)], axis=0
    )
    down_local = down_weight[0]
    gate_local = gate_weight[0]
    up_local = up_weight[0]
    width = padded.shape[1] // lax.axis_size("tp")
    own = lax.dynamic_slice_in_dim(padded, lax.axis_index("tp") * width, width, 1)
    outgoing = own[source].reshape(experts, capacity, width)
    received = lax.all_to_all(outgoing, "ep", split_axis=0, concat_axis=0, tiled=True)
    flat = received.reshape(experts * capacity, width)
    head_piece = lax.all_gather(mixed, "tp", axis=1, tiled=True)
    feature_piece = lax.all_gather(flat, "tp", axis=1, tiled=True)
    mixer_total = add_product(head_piece, output_weight)
    gate = add_product(feature_piece, gate_local)
    up = add_product(feature_piece, up_local)
    hidden = activate(gate, up)
    result = add_product(lax.all_gather(hidden, "tp", axis=1, tiled=True), down_local)
    result = result.astype(jnp.bfloat16).reshape(experts, capacity, down_local.shape[1])
    returned = lax.all_to_all(result, "ep", split_axis=0, concat_axis=0, tiled=True)
    mixer_output = mixer_total.astype(jnp.bfloat16)
    results = returned.reshape(experts * capacity, returned.shape[2])
    picked = results[target].astype(jnp.float32).reshape(rows_here, TOP_K, returned.shape[2])
    expert_output = jnp.sum(picked * chances[:, :, None], axis=1).astype(jnp.bfloat16)
    return (mixer_output, expert_output)


def solution(mesh):
    return jax.shard_map(
        shards,
        mesh=mesh,
        in_specs=(
            P("ep", None),
            P(),
            P(None, "tp"),
            P(None, "tp"),
            P(None, "tp"),
            P(None, "tp"),
            P("tp"),
            P("ep", None),
            P(),
            P("ep", None),
            P("ep", None),
            P("ep", None, "tp"),
            P("ep", None, "tp"),
            P("ep", None, "tp"),
        ),
        out_specs=(P("ep", "tp"), P("ep", "tp")),
        check_vma=False,
    )
```

profile of v0, /device:TPU:0, one launch (start us, length us, event | category | flops | bytes accessed | tf_op | source)
XLA Modules:
  0.0 214.6 jit_solution(16968832232059653629)
XLA Ops:
  9.1 1.2 fusion.19
  10.3 1.1 reduce-window.6
  12.0 2.4 %scatter_custom_fusion = s32[1024]{0:T(1024)S(1)} fusion(s32[512]{0:T(512)S(1)} %bitcast.98, s32[512]{0:T(512)S(1)} %add_select_fusion, s32[]{:T(128)} %constant.101.clone.1), kind=kCustom, calls=%fused_computation.95 | custom fusion | bytes 4100 | tf_op jit(solution)/shard_map/scatter | solution.py:147
  14.5 1.2 fusion.21
  15.8 4.0 %gather_fusion = bf16[1024,512]{1,0:T(8,128)(2,1)S(1)} fusion(bf16[129,512]{1,0:T(8,128)(2,1)S(1)} %pad_dynamic-slice_fusion, s32[1024]{0:T(1024)S(1)} %fusion.37), kind=kCustom, calls=%fused_computation | custom fusion | bytes 2101248 | tf_op jit(solution)/shard_map/gather | solution.py:157
  19.7 32.8 %all_to_all.10 = bf16[8,128,512]{2,1,0:T(8,128)(2,1)} all-to-all(bf16[8,128,512]{2,1,0:T(8,128)(2,1)S(1)} %bitcast.89), channel_id=1, replica_groups=mesh['ep'=8,'tp'=4] {'ep'}, dimensions={0} | all-to-all | bytes 2097152 | tf_op jit(solution)/shard_map/all_to_all | solution.py:158
  52.6 51.5 %all-gather.6.cloned.1.call-done = bf16[1024,2048]{1,0:T(8,128)(2,1)} async-done(((bf16[1024,512]{1,0:T(8,128)(2,1)}), bf16[1024,2048]{1,0:T(8,128)(2,1)}) %all-gather.6.cloned.1.call-update) | async-done | bytes 4194320 | tf_op jit(solution)/shard_map/all_gather | solution.py:161
  104.1 4.7 %fusion.7 = f32[1024,512]{1,0:T(8,128)S(1)} fusion(bf16[1024,2048]{1,0:T(8,128)(2,1)} %all-gather.6.cloned.1.call-done, bf16[1,2048,512]{2,1,0:T(8,128)(2,1)S(1)} %copy-done), kind=kOutput, calls=%fused_computation.15 | convolution fusion | flops 2147483648 | bytes 8388608 | tf_op jit(solution)/shard_map/dot_general | solution.py:66
  108.8 3.8 %multiply_convert_fusion = bf16[1024,512]{1,0:T(8,128)(2,1)} fusion(f32[1024,512]{1,0:T(8,128)S(1)} %fusion.7, bf16[1024,2048]{1,0:T(8,128)(2,1)S(1)} %copy-done.4, bf16[1,2048,512]{2,1,0:T(8,128)(2,1)S(1)} %copy-done.5), kind=kOutput, calls=%fused_computation.19 | convolution fusion | flops 2152726528 | bytes 9437184 | tf_op jit(solution)/shard_map/dot_general | solution.py:66
  113.4 1.9 fusion.56
  116.8 2.2 %collective-permute-start = (bf16[128,512]{0,1:T(8,128)(2,1)}, bf16[128,512]{0,1:T(8,128)(2,1)}, u32[]{:S(2)}, u32[]{:S(2)}) collective-permute-start(bf16[128,512]{0,1:T(8,128)(2,1)} %get-tuple-element.16), channel_id=1, source_target_pairs={{0,4},{4,8},{8,12},{12,16},{16,20},{20,24},{24,28},{1,5},{5,9},{9,... | collective-permute-start | bytes 393224 | tf_op jit(solution)/shard_map/ppermute | solution.py:23
  119.0 1.6 collective-permute-start.1
  120.6 1.1 fusion.53
  125.1 1.0 pad_maximum_fusion.1
  126.6 1.6 fusion.1
  131.1 34.2 %all-gather.8.cloned.1.call-done = bf16[1024,2048]{1,0:T(8,128)(2,1)} async-done(((bf16[1024,512]{1,0:T(8,128)(2,1)}), bf16[1024,2048]{1,0:T(8,128)(2,1)}) %all-gather.8.cloned.1.call-update) | async-done | bytes 4194320 | tf_op jit(solution)/shard_map/all_gather | solution.py:166
  165.3 6.2 %fusion.14 = bf16[1024,512]{1,0:T(8,128)(2,1)} fusion(bf16[1024,2048]{1,0:T(8,128)(2,1)} %all-gather.8.cloned.1.call-done, bf16[1,2048,512]{2,1,0:T(8,128)(2,1)} %param.27), kind=kOutput, calls=%fused_computation.21 | convolution fusion | flops 2148007936 | bytes 7340032 | tf_op jit(solution)/shard_map/dot_general | solution.py:66
  171.5 4.7 %all-to-all-start.1 = ((bf16[8,128,512]{2,1,0:T(8,128)(2,1)}), bf16[8,128,512]{2,1,0:T(8,128)(2,1)S(1)}, u32[]{:S(2)}, u32[]{:S(2)}) async-start(bf16[8,128,512]{2,1,0:T(8,128)(2,1)} %bitcast.93), calls=%async_computation.1 | async-start | bytes 2097152 | tf_op jit(solution)/shard_map/all_to_all | solution.py:168
  176.4 17.9 %all-gather.4.cloned.1.call-done = bf16[256,2048]{0,1:T(8,128)(2,1)} async-done(((bf16[256,512]{0,1:T(8,128)(2,1)}), bf16[256,2048]{0,1:T(8,128)(2,1)}) %all-gather.4.cloned.1.call-update) | async-done | bytes 1048592 | tf_op jit(solution)/shard_map/all_gather | solution.py:160
  194.2 3.3 %convolution_convert_fusion = bf16[256,512]{1,0:T(8,128)(2,1)} fusion(bf16[256,2048]{0,1:T(8,128)(2,1)} %all-gather.4.cloned.1.call-done, bf16[2048,512]{1,0:T(8,128)(2,1)} %param.19), kind=kOutput, calls=%fused_computation.24 | convolution fusion | flops 537001984 | bytes 3407872 | tf_op jit(solution)/shard_map/dot_general | solution.py:66
  197.6 5.2 %all-to-all-done.1 = bf16[8,128,512]{2,1,0:T(8,128)(2,1)S(1)} async-done(((bf16[8,128,512]{2,1,0:T(8,128)(2,1)}), bf16[8,128,512]{2,1,0:T(8,128)(2,1)S(1)}, u32[]{:S(2)}, u32[]{:S(2)}) %all-to-all-start.1) | async-done | bytes 1048608 | tf_op jit(solution)/shard_map/all_to_all | solution.py:168
  202.8 2.6 %gather_fusion.1 = bf16[512,512]{1,0:T(8,128)(2,1)} fusion(bf16[1024,512]{1,0:T(8,128)(2,1)S(1)} %bitcast.88, s32[1024]{0:T(1024)S(1)} %pad_clamp_fusion), kind=kCustom, calls=%fused_computation.1 | custom fusion | bytes 1050624 | tf_op jit(solution)/shard_map/gather | solution.py:171
  205.4 1.4 reshape.338
  206.7 1.4 multiply_reduce_fusion
  (83 shorter events, 11.5 us)
Async XLA Ops:
  7.2 97.0 %copy-start = (bf16[1,2048,512]{2,1,0:T(8,128)(2,1)S(1)}, bf16[1,2048,512]{2,1,0:T(8,128)(2,1)}, u32[]{:S(2)}) copy-start(bf16[1,2048,512]{2,1,0:T(8,128)(2,1)} %param.26) | copy-start | bytes 6291460
  7.2 96.9 %all-gather.6.cloned.1.call-start = ((), (), s32[]{:S(2)}) async-start(), calls=%async_computation.3 | async-start | bytes 5242880 | tf_op jit(solution)/shard_map/all_gather | solution.py:161
  52.6 112.7 %all-gather.8.cloned.1.call-start = ((), (), s32[]{:S(2)}) async-start(), calls=%async_computation.4 | async-start | bytes 5242880 | tf_op jit(solution)/shard_map/all_gather | solution.py:166
  104.1 4.7 %copy-start.4 = (bf16[1024,2048]{1,0:T(8,128)(2,1)S(1)}, bf16[1024,2048]{1,0:T(8,128)(2,1)}, u32[]{:S(2)}) copy-start(bf16[1024,2048]{1,0:T(8,128)(2,1)} %all-gather.6.cloned.1.call-done) | copy-start | bytes 12582916
  104.1 4.7 %copy-start.5 = (bf16[1,2048,512]{2,1,0:T(8,128)(2,1)S(1)}, bf16[1,2048,512]{2,1,0:T(8,128)(2,1)}, u32[]{:S(2)}) copy-start(bf16[1,2048,512]{2,1,0:T(8,128)(2,1)} %param.25) | copy-start | bytes 6291460
  108.8 4.0 %copy-start.1 = (bf16[256,2048]{1,0:T(8,128)(2,1)S(1)}, bf16[256,2048]{1,0:T(8,128)(2,1)}, u32[]{:S(2)}) copy-start(bf16[256,2048]{1,0:T(8,128)(2,1)} %param.14) | copy-start | bytes 3145732
  112.7 0.7 copy-start.8
  112.7 81.5 %all-gather.4.cloned.1.call-start = ((), (), s32[]{:S(2)}) async-start(), calls=%async_computation.2 | async-start | bytes 1310720 | tf_op jit(solution)/shard_map/all_gather | solution.py:160
  113.1 2.3 %copy-start.7 = (bf16[2048,256]{1,0:T(8,128)(2,1)S(1)}, bf16[2048,256]{1,0:T(8,128)(2,1)}, u32[]{:S(2)}) copy-start(bf16[2048,256]{1,0:T(8,128)(2,1)} %param.18) | copy-start | bytes 3145732
  115.3 5.3 %copy-start.6 = (bf16[2048,512]{1,0:T(8,128)(2,1)S(1)}, bf16[2048,512]{1,0:T(8,128)(2,1)}, u32[]{:S(2)}) copy-start(bf16[2048,512]{1,0:T(8,128)(2,1)} %param.16) | copy-start | bytes 6291460
  116.8 8.3 %collective-permute-start = (bf16[128,512]{0,1:T(8,128)(2,1)}, bf16[128,512]{0,1:T(8,128)(2,1)}, u32[]{:S(2)}, u32[]{:S(2)}) collective-permute-start(bf16[128,512]{0,1:T(8,128)(2,1)} %get-tuple-element.16), channel_id=1, source_target_pairs={{0,4},{4,8},{8,12},{12,16},{16,20},{20,24},{24,28},{1,5},{5,9},{9,... | collective-permute-start | bytes 393224 | tf_op jit(solution)/shard_map/ppermute | solution.py:23
  119.0 5.4 %copy-start.3 = (f32[8]{0:T(128)S(1)}, f32[8]{0:T(128)}, u32[]{:S(2)}) copy-start(f32[8]{0:T(128)} %param.20) | copy-start | bytes 100
  119.0 6.1 %collective-permute-start.1 = (bf16[128,512]{0,1:T(8,128)(2,1)}, bf16[128,512]{0,1:T(8,128)(2,1)}, u32[]{:S(2)}, u32[]{:S(2)}) collective-permute-start(bf16[128,512]{0,1:T(8,128)(2,1)} %get-tuple-element.15), channel_id=1, source_target_pairs={{4,0},{8,4},{12,8},{16,12},{20,16},{24,20},{28,24},{5,1},{9,5},{13... | collective-permute-start | bytes 393224 | tf_op jit(solution)/shard_map/ppermute | solution.py:24
  171.5 4.7 %copy-start.2 = (f32[128,4]{0,1:T(4,128)S(1)}, f32[128,4]{0,1:T(4,128)}, u32[]{:S(2)}) copy-start(f32[128,4]{0,1:T(4,128)} %param.24) | copy-start | bytes 6148
  171.5 31.3 %all-to-all-start.1 = ((bf16[8,128,512]{2,1,0:T(8,128)(2,1)}), bf16[8,128,512]{2,1,0:T(8,128)(2,1)S(1)}, u32[]{:S(2)}, u32[]{:S(2)}) async-start(bf16[8,128,512]{2,1,0:T(8,128)(2,1)} %bitcast.93), calls=%async_computation.1 | async-start | bytes 2097152 | tf_op jit(solution)/shard_map/all_to_all | solution.py:168
Sparse Core Ops, SparseCore 0:
  52.7 51.3 all-gather.5
  112.8 52.4 all-gather.7
  167.7 26.4 all-gather.3
where the time goes:
time: 215 us
  waiting for transfers between devices  109 us (51%)
  blocking collectives  32.8 us (15%)
  matrix products  24.2 us (11%)
  local copies, waits for them, and re-layouts  16.3 us (8%)
  between operations  14.1 us (7%)
  other arithmetic  9.73 us (5%)
  starting transfers between devices  8.66 us (4%)
    all_gather x1, waiting for transfers between devices, shards(): feature_piece = lax.all_gather(flat, 'tp', axis=1, tiled=True)  51.5 us
    all_gather x1, waiting for transfers between devices, shards(): lax.all_gather(hidden, 'tp', axis=1, tiled=True)  34.2 us
    all_to_all x1, blocking collectives, shards(): lax.all_to_all(outgoing, 'ep', split_axis=0, concat_axis=0, tiled=True)  32.8 us
    dot_general x4, matrix products, add_product(): return jnp.dot(piece, weight, preferred_element_type=jnp.float32)  18 us
    all_gather x1, waiting for transfers between devices, shards(): head_piece = lax.all_gather(mixed, 'tp', axis=1, tiled=True)  17.9 us
    all_to_all x1, waiting for transfers between devices, shards(): lax.all_to_all(result, 'ep', split_axis=0, concat_axis=0, tiled=True)  5.17 us
    all_to_all x1, starting transfers between devices, shards(): lax.all_to_all(result, 'ep', split_axis=0, concat_axis=0, tiled=True)  4.74 us
  transfers between devices with their start and end apart: 6, of which 4 were waited for; matrix products, arithmetic and copies ran while one was open for 11% of the time, Pallas kernels for 0%

commit v1 on v0

--- a/solution.py
+++ b/solution.py
@@ -158,7 +158,12 @@
     received = lax.all_to_all(outgoing, "ep", split_axis=0, concat_axis=0, tiled=True)
     flat = received.reshape(experts * capacity, width)
     head_piece = lax.all_gather(mixed, "tp", axis=1, tiled=True)
-    feature_piece = lax.all_gather(flat, "tp", axis=1, tiled=True)
+    ring = [flat]
+    for hop in range(3):
+        ring.append(lax.ppermute(ring[-1], "tp", [(dev, (dev + 1) % 4) for dev in range(4)]))
+    feature_piece = jnp.roll(
+        jnp.concatenate(ring[::-1], axis=1), (lax.axis_index("tp") + 1) * ring[0].shape[1], axis=1
+    )
     mixer_total = add_product(head_piece, output_weight)
     gate = add_product(feature_piece, gate_local)
     up = add_product(feature_piece, up_local)

time: 215 us -> 244 us (1.13)
  waiting for transfers between devices: 109 us -> 130 us
  local copies, waits for them, and re-layouts: 16.3 us -> 25 us
  matrix products: 24.2 us -> 21 us
    ppermute x0 -> x3, waiting for transfers between devices: none -> 72.1 us  [shards(): lax.ppermute(ring[-1], 'tp', [(dev, (dev + 1) % 4) for dev in range(4)])]
    all_gather x1 -> x0, waiting for transfers between devices: 51.5 us -> none  [shards(): feature_piece = lax.all_gather(flat, 'tp', axis=1, tiled=True)]
    unnamed x22 -> x39, local copies, waits for them, and re-layouts: 1.9 us -> 9.3 us
  transfers between devices with their start and end apart: 6 -> 8, of which waited for: 4 -> 6; matrix products, arithmetic and copies ran while one was open for 11% -> 10% of each run, Pallas kernels for 0% -> 0%
where the time goes in v1:
time: 244 us; the launch traced here: 243 us
  waiting for transfers between devices  130 us (53%)
  blocking collectives  32.9 us (13%)
  local copies, waits for them, and re-layouts  25 us (10%)
  matrix products  21 us (9%)
  between operations  14.5 us (6%)
  starting transfers between devices  10.3 us (4%)
  other arithmetic  9.73 us (4%)
    ppermute x3, waiting for transfers between devices, shards(): lax.ppermute(ring[-1], 'tp', [(dev, (dev + 1) % 4) for dev in range(4)])  72.1 us
    all_gather x1, waiting for transfers between devices, shards(): lax.all_gather(hidden, 'tp', axis=1, tiled=True)  34.6 us
    all_to_all x1, blocking collectives, shards(): lax.all_to_all(outgoing, 'ep', split_axis=0, concat_axis=0, tiled=True)  32.9 us
    all_gather x1, waiting for transfers between devices, shards(): head_piece = lax.all_gather(mixed, 'tp', axis=1, tiled=True)  18 us
    dot_general x4, matrix products, add_product(): return jnp.dot(piece, weight, preferred_element_type=jnp.float32)  15.6 us
    unnamed x39, local copies, waits for them, and re-layouts  9.3 us
    gather x1, local copies, waits for them, and re-layouts, shards(): outgoing = own[source].reshape(experts, capacity, width)  5.08 us
    all_to_all x1, waiting for transfers between devices, shards(): lax.all_to_all(result, 'ep', split_axis=0, concat_axis=0, tiled=True)  5.04 us
  transfers between devices with their start and end apart: 8, of which 6 were waited for; matrix products, arithmetic and copies ran while one was open for 10% of the time, Pallas kernels for 0%

profile of v1, /device:TPU:0, one launch (start us, length us, event | category | flops | bytes accessed | tf_op | source)
XLA Modules:
  0.0 243.2 jit_solution(11483940394623511079)
XLA Ops:
  12.0 2.4 %scatter_custom_fusion = s32[1024]{0:T(1024)S(1)} fusion(s32[512]{0:T(512)S(1)} %bitcast.98, s32[512]{0:T(512)S(1)} %add_select_fusion, s32[]{:T(128)} %constant.120.clone.1), kind=kCustom, calls=%fused_computation.105 | custom fusion | bytes 4100 | tf_op jit(solution)/shard_map/scatter | solution.py:147
  15.8 5.1 %gather_fusion = bf16[1024,512]{1,0:T(8,128)(2,1)} fusion(bf16[129,512]{1,0:T(8,128)(2,1)S(1)} %pad_dynamic-slice_fusion, s32[1024]{0:T(1024)S(1)} %fusion.41), kind=kCustom, calls=%fused_computation | custom fusion | bytes 2101248 | tf_op jit(solution)/shard_map/gather | solution.py:157
  20.9 32.9 %all_to_all.10 = bf16[8,128,512]{2,1,0:T(8,128)(2,1)S(1)} all-to-all(bf16[8,128,512]{2,1,0:T(8,128)(2,1)} %bitcast.90), channel_id=1, replica_groups=mesh['ep'=8,'tp'=4] {'ep'}, dimensions={0} | all-to-all | bytes 2097152 | tf_op jit(solution)/shard_map/all_to_all | solution.py:158
  53.8 1.5 collective-permute-start.2
  55.3 23.9 %collective-permute-done.2 = bf16[1024,512]{1,0:T(8,128)(2,1)S(1)} collective-permute-done((bf16[1024,512]{1,0:T(8,128)(2,1)S(1)}, bf16[1024,512]{1,0:T(8,128)(2,1)S(1)}, u32[]{:S(2)}, u32[]{:S(2)}) %collective-permute-start.2) | collective-permute-done | bytes 1048608 | tf_op jit(solution)/shard_map/ppermute | solution.py:163
  80.8 24.1 %collective-permute-done.3 = bf16[1024,512]{1,0:T(8,128)(2,1)} collective-permute-done((bf16[1024,512]{1,0:T(8,128)(2,1)S(1)}, bf16[1024,512]{1,0:T(8,128)(2,1)}, u32[]{:S(2)}, u32[]{:S(2)}) %collective-permute-start.3) | collective-permute-done | bytes 1048608 | tf_op jit(solution)/shard_map/ppermute | solution.py:163
  104.9 24.0 %collective-permute-done.4 = bf16[1024,512]{1,0:T(8,128)(2,1)} collective-permute-done((bf16[1024,512]{1,0:T(8,128)(2,1)}, bf16[1024,512]{1,0:T(8,128)(2,1)}, u32[]{:S(2)}, u32[]{:S(2)}) %collective-permute-start.4) | collective-permute-done | bytes 1048608 | tf_op jit(solution)/shard_map/ppermute | solution.py:163
  128.9 1.4 constant_dynamic-update-slice_fusion.7
  130.3 1.4 constant_dynamic-update-slice_fusion.6
  132.0 1.4 constant_dynamic-update-slice_fusion.3
  133.4 1.4 constant_dynamic-update-slice_fusion.2
  135.2 2.3 fusion.2
  137.5 3.8 %multiply_convert_fusion = bf16[1024,512]{1,0:T(8,128)(2,1)} fusion(f32[1024,512]{1,0:T(8,128)S(1)} %fusion.2, bf16[1,2048,512]{2,1,0:T(8,128)(2,1)S(1)} %copy-done.10, bf16[1024,4096]{1,0:T(8,128)(2,1)S(1)} %constant_dynamic-update-slice_fusion, s32[]{:T(128)S(6)} %select_n.69), kind=kOutput, calls=%fused_computation.21 | convolution fusion | flops 2152726528 | bytes 9437188 | tf_op jit(solution)/shard_map/dot_general | solution.py:66
  141.9 2.0 fusion.62
  145.5 2.1 collective-permute-start
  147.5 1.5 collective-permute-start.1
  159.1 34.6 %all-gather.5.cloned.1.call-done = bf16[1024,2048]{1,0:T(8,128)(2,1)} async-done(((bf16[1024,512]{1,0:T(8,128)(2,1)}), bf16[1024,2048]{1,0:T(8,128)(2,1)}) %all-gather.5.cloned.1.call-update) | async-done | bytes 4194320 | tf_op jit(solution)/shard_map/all_gather | solution.py:171
  193.7 6.2 %fusion.18 = bf16[1024,512]{1,0:T(8,128)(2,1)} fusion(bf16[1024,2048]{1,0:T(8,128)(2,1)} %all-gather.5.cloned.1.call-done, bf16[1,2048,512]{2,1,0:T(8,128)(2,1)} %param.27), kind=kOutput, calls=%fused_computation.23 | convolution fusion | flops 2148007936 | bytes 7340032 | tf_op jit(solution)/shard_map/dot_general | solution.py:66
  199.8 4.6 %all-to-all-start.1 = ((bf16[8,128,512]{2,1,0:T(8,128)(2,1)}), bf16[8,128,512]{2,1,0:T(8,128)(2,1)S(1)}, u32[]{:S(2)}, u32[]{:S(2)}) async-start(bf16[8,128,512]{2,1,0:T(8,128)(2,1)} %bitcast.93), calls=%async_computation.1 | async-start | bytes 2097152 | tf_op jit(solution)/shard_map/all_to_all | solution.py:173
  204.6 18.0 %all-gather.3.cloned.1.call-done = bf16[256,2048]{0,1:T(8,128)(2,1)} async-done(((bf16[256,512]{0,1:T(8,128)(2,1)}), bf16[256,2048]{0,1:T(8,128)(2,1)}) %all-gather.3.cloned.1.call-update) | async-done | bytes 1048592 | tf_op jit(solution)/shard_map/all_gather | solution.py:160
  222.6 3.3 %convolution_convert_fusion = bf16[256,512]{1,0:T(8,128)(2,1)} fusion(bf16[256,2048]{0,1:T(8,128)(2,1)} %all-gather.3.cloned.1.call-done, bf16[2048,512]{1,0:T(8,128)(2,1)} %param.19), kind=kOutput, calls=%fused_computation.26 | convolution fusion | flops 537001984 | bytes 3407872 | tf_op jit(solution)/shard_map/dot_general | solution.py:66
  226.0 5.0 %all-to-all-done.1 = bf16[8,128,512]{2,1,0:T(8,128)(2,1)S(1)} async-done(((bf16[8,128,512]{2,1,0:T(8,128)(2,1)}), bf16[8,128,512]{2,1,0:T(8,128)(2,1)S(1)}, u32[]{:S(2)}, u32[]{:S(2)}) %all-to-all-start.1) | async-done | bytes 1048608 | tf_op jit(solution)/shard_map/all_to_all | solution.py:173
  231.0 2.6 %gather_fusion.1 = bf16[512,512]{1,0:T(8,128)(2,1)} fusion(bf16[1024,512]{1,0:T(8,128)(2,1)S(1)} %bitcast.86, s32[1024]{0:T(1024)S(1)} %pad_clamp_fusion), kind=kCustom, calls=%fused_computation.1 | custom fusion | bytes 1050624 | tf_op jit(solution)/shard_map/gather | solution.py:176
  233.6 1.4 reshape.338
  (104 shorter events, 21.9 us)
Async XLA Ops:
  7.2 128.0 %copy-start = (bf16[1,2048,512]{2,1,0:T(8,128)(2,1)S(1)}, bf16[1,2048,512]{2,1,0:T(8,128)(2,1)}, u32[]{:S(2)}) copy-start(bf16[1,2048,512]{2,1,0:T(8,128)(2,1)} %param.25) | copy-start | bytes 6291460
  7.2 186.5 %all-gather.5.cloned.1.call-start = ((), (), s32[]{:S(2)}) async-start(), calls=%async_computation.3 | async-start | bytes 5242880 | tf_op jit(solution)/shard_map/all_gather | solution.py:171
  53.8 25.4 %collective-permute-start.2 = (bf16[1024,512]{1,0:T(8,128)(2,1)S(1)}, bf16[1024,512]{1,0:T(8,128)(2,1)S(1)}, u32[]{:S(2)}, u32[]{:S(2)}) collective-permute-start(bf16[1024,512]{1,0:T(8,128)(2,1)S(1)} %bitcast.87), channel_id=1, source_target_pairs={{0,1},{1,2},{2,3},{3,0},{4,5},{5,6},{6,7},{7,4},{8,9},{9,10},{10,1... | collective-permute-start | bytes 3145736 | tf_op jit(solution)/shard_map/ppermute | solution.py:163
  79.2 1.0 copy-start.1
  80.2 24.7 %collective-permute-start.3 = (bf16[1024,512]{1,0:T(8,128)(2,1)S(1)}, bf16[1024,512]{1,0:T(8,128)(2,1)}, u32[]{:S(2)}, u32[]{:S(2)}) collective-permute-start(bf16[1024,512]{1,0:T(8,128)(2,1)S(1)} %collective-permute-done.2), channel_id=1, source_target_pairs={{0,1},{1,2},{2,3},{3,0},{4,5},{5,6},{6,7},{7,4},{8,9},{9,10},{10,1... | collective-permute-start | bytes 3145736 | tf_op jit(solution)/shard_map/ppermute | solution.py:163
  104.9 24.0 %collective-permute-start.4 = (bf16[1024,512]{1,0:T(8,128)(2,1)}, bf16[1024,512]{1,0:T(8,128)(2,1)}, u32[]{:S(2)}, u32[]{:S(2)}) collective-permute-start(bf16[1024,512]{1,0:T(8,128)(2,1)} %collective-permute-done.3), channel_id=1, source_target_pairs={{0,1},{1,2},{2,3},{3,0},{4,5},{5,6},{6,7},{7,4},{8,9},{9,10},{10,1... | collective-permute-start | bytes 3145736 | tf_op jit(solution)/shard_map/ppermute | solution.py:163
  104.9 26.8 %copy-start.2 = (bf16[1024,512]{1,0:T(8,128)(2,1)S(1)}, bf16[1024,512]{1,0:T(8,128)(2,1)}, u32[]{:S(2)}) copy-start(bf16[1024,512]{1,0:T(8,128)(2,1)} %copy-done.1) | copy-start | bytes 3145732
  135.1 2.3 copy-start.10
  137.5 3.9 %copy-start.3 = (bf16[256,2048]{1,0:T(8,128)(2,1)S(1)}, bf16[256,2048]{1,0:T(8,128)(2,1)}, u32[]{:S(2)}) copy-start(bf16[256,2048]{1,0:T(8,128)(2,1)} %param.14) | copy-start | bytes 3145732
  137.5 4.4 %copy-start.13 = (f32[2048]{0:T(1024)S(1)}, f32[2048]{0:T(1024)}, u32[]{:S(2)}) copy-start(f32[2048]{0:T(1024)} %param.15) | copy-start | bytes 24580
  141.3 81.3 %all-gather.3.cloned.1.call-start = ((), (), s32[]{:S(2)}) async-start(), calls=%async_computation.2 | async-start | bytes 1310720 | tf_op jit(solution)/shard_map/all_gather | solution.py:160
  141.4 2.7 %copy-start.12 = (bf16[2048,256]{1,0:T(8,128)(2,1)S(1)}, bf16[2048,256]{1,0:T(8,128)(2,1)}, u32[]{:S(2)}) copy-start(bf16[2048,256]{1,0:T(8,128)(2,1)} %param.18) | copy-start | bytes 3145732
  141.9 7.1 %copy-start.11 = (bf16[2048,512]{1,0:T(8,128)(2,1)S(1)}, bf16[2048,512]{1,0:T(8,128)(2,1)}, u32[]{:S(2)}) copy-start(bf16[2048,512]{1,0:T(8,128)(2,1)} %param.16) | copy-start | bytes 6291460
  145.5 7.4 %copy-start.9 = (f32[8]{0:T(128)S(1)}, f32[8]{0:T(128)}, u32[]{:S(2)}) copy-start(f32[8]{0:T(128)} %param.20) | copy-start | bytes 100
  145.5 8.1 %collective-permute-start = (bf16[128,512]{0,1:T(8,128)(2,1)}, bf16[128,512]{0,1:T(8,128)(2,1)}, u32[]{:S(2)}, u32[]{:S(2)}) collective-permute-start(bf16[128,512]{0,1:T(8,128)(2,1)} %get-tuple-element.16), channel_id=1, source_target_pairs={{0,4},{4,8},{8,12},{12,16},{16,20},{20,24},{24,28},{1,5},{5,9},{9,... | collective-permute-start | bytes 393224 | tf_op jit(solution)/shard_map/ppermute | solution.py:23
  147.5 6.0 %collective-permute-start.1 = (bf16[128,512]{0,1:T(8,128)(2,1)}, bf16[128,512]{0,1:T(8,128)(2,1)}, u32[]{:S(2)}, u32[]{:S(2)}) collective-permute-start(bf16[128,512]{0,1:T(8,128)(2,1)} %get-tuple-element.15), channel_id=1, source_target_pairs={{4,0},{8,4},{12,8},{16,12},{20,16},{24,20},{28,24},{5,1},{9,5},{13... | collective-permute-start | bytes 393224 | tf_op jit(solution)/shard_map/ppermute | solution.py:24
  154.6 0.8 copy-start.4
  154.6 0.9 copy-start.5
  154.6 0.9 copy-start.6
  154.7 0.9 copy-start.7
  159.1 45.4 %copy-start.8 = (f32[128,4]{0,1:T(4,128)S(1)}, f32[128,4]{0,1:T(4,128)}, u32[]{:S(2)}) copy-start(f32[128,4]{0,1:T(4,128)} %param.24) | copy-start | bytes 6148
  199.8 31.2 %all-to-all-start.1 = ((bf16[8,128,512]{2,1,0:T(8,128)(2,1)}), bf16[8,128,512]{2,1,0:T(8,128)(2,1)S(1)}, u32[]{:S(2)}, u32[]{:S(2)}) async-start(bf16[8,128,512]{2,1,0:T(8,128)(2,1)} %bitcast.93), calls=%async_computation.1 | async-start | bytes 2097152 | tf_op jit(solution)/shard_map/all_to_all | solution.py:173
Sparse Core Ops, SparseCore 0:
  141.4 52.2 all-gather.4
  196.1 26.4 all-gather.2
